TPU v7x, 32 devices: a whole 2x2x4 slice. The times are simulated.
32 devices in a mesh: grp: 2 (over y), sp: 4 (over z), dp: 4 (over x, core).
Axes of the slice: x: 2, y: 2, z: 4, core: 2. Of those that a mesh axis runs over, the one named last changes fastest.
Arguments:
- queries: bfloat16 [8, 512, 16, 192], P(('grp', 'dp'), 'sp'), parts along dimension 0, may hold values from -41 to 41
- kv_latent: bfloat16 [8, 512, 512], P(('grp', 'dp'), 'sp'), parts along dimension 0, may hold values from -6 to 6
- rope_key: bfloat16 [8, 512, 64], P(('grp', 'dp'), 'sp'), parts along dimension 0, may hold values from -5.1 to 5.1
- kv_gain: float32 [512], replicated, may hold values from 0.1 to 1.9
- kv_weight: bfloat16 [512, 4096], P('dp', 'sp'), may hold values from -0.25 to 0.25
- out_weight: bfloat16 [2048, 2048], P(None, 'dp'), may hold values from -1 to 1
Outputs:
- mixed: bfloat16 [8, 512, 2048], P(('grp', 'dp'), 'sp'), parts along dimension 0
There are 2 independent parts, one for each index of `grp`. A program takes and returns all parts, laid end to end along the dimension named above; an argument that names none is the same for every part. Nothing has to cross between parts.
All inputs are finite; a program needn't handle non-finite values.
Results may differ from a plain program's by a relative error of at most 0.0075.
Values may be sent and summed in bfloat16 or wider, within the bound.
A program may use at most 64 MiB of HBM per device.

v0:
```python
import jax
import jax.numpy as jnp
from jax import lax
from jax.sharding import PartitionSpec as P

NOPE = 128
VD = 128


def rotate(values, positions):
    half = values.shape[-1] // 2
    inverse = jnp.power(10000.0, -jnp.arange(half, dtype=jnp.float32) * 2.0 / values.shape[-1])
    angle = positions.astype(jnp.float32)[..., None] * inverse
    first = values[..., :half].astype(jnp.float32)
    second = values[..., half:].astype(jnp.float32)
    cosine = jnp.cos(angle)
    sine = jnp.sin(angle)
    return jnp.concatenate(
        [first * cosine - second * sine, first * sine + second * cosine], axis=-1
    )


def attend(query_rot, key_value, key_rot):
    length, heads = (query_rot.shape[0], query_rot.shape[1])
    nope = query_rot.shape[2] - key_rot.shape[1]
    scale = query_rot.shape[2] ** (-0.5)
    content = key_value[:, :, :nope]
    values = key_value[:, :, nope:]
    shared = jnp.broadcast_to(key_rot[:, None, :], (length, heads, key_rot.shape[1]))
    keys = jnp.concatenate([content, shared], axis=-1)
    block = min(512, length)
    blocks = query_rot.reshape(length // block, block, heads, query_rot.shape[2])
    key_pos = jnp.arange(length, dtype=jnp.int32)

    def one_block(item):
        query_block, index = item
        scores = (
            jnp.einsum("qhd,khd->hqk", query_block, keys, preferred_element_type=jnp.float32)
            * scale
        )
        query_pos = index * block + jnp.arange(block, dtype=jnp.int32)
        kept = query_pos[:, None] >= key_pos[None, :]
        scores = jnp.where(kept[None], scores, -jnp.inf)
        top = jnp.max(scores, axis=-1, keepdims=True)
        expo = jnp.exp(scores - top)
        probs = (expo / jnp.sum(expo, axis=-1, keepdims=True)).astype(jnp.bfloat16)
        return jnp.einsum("hqk,khd->qhd", probs, values, preferred_element_type=jnp.float32).astype(
            jnp.bfloat16
        )

    result = lax.map(one_block, (blocks, jnp.arange(length // block, dtype=jnp.int32)))
    return result.reshape(length, heads, values.shape[2])


def body(queries, kv_latent, rope_key, kv_gain, kv_weight, out_weight):
    tok_rows = queries.shape[1]
    positions = lax.axis_index("sp") * tok_rows + jnp.arange(tok_rows, dtype=jnp.int32)
    latent32 = kv_latent[0].astype(jnp.float32)
    latent_n = (
        latent32
        * lax.rsqrt(jnp.mean(latent32 * latent32, axis=-1, keepdims=True) + 1e-06)
        * kv_gain
    ).astype(jnp.bfloat16)
    key_rot = rotate(rope_key[0], positions).astype(jnp.bfloat16)
    turned = rotate(queries[0, :, :, NOPE:], positions[:, None])
    query_rot = jnp.concatenate(
        [queries[0, :, :, :NOPE].astype(jnp.float32), turned], axis=-1
    ).astype(jnp.bfloat16)
    query_heads = lax.all_to_all(query_rot[None], "sp", split_axis=2, concat_axis=1, tiled=True)
    every_latent, every_key = (
        lax.all_gather(latent_n[None], "sp", axis=1, tiled=True),
        lax.all_gather(key_rot[None], "sp", axis=1, tiled=True),
    )
    whole_latent = every_latent[0]
    kv_heads = jnp.dot(
        whole_latent,
        lax.all_gather(kv_weight, "dp", axis=0, tiled=True),
        preferred_element_type=jnp.float32,
    ).astype(jnp.bfloat16)
    kv_heads = kv_heads.reshape(whole_latent.shape[0], kv_weight.shape[1] // (NOPE + VD), NOPE + VD)
    attended = attend(query_heads[0], kv_heads, every_key[0])
    returned = lax.all_to_all(attended[None], "sp", split_axis=1, concat_axis=2, tiled=True)
    flat_rows = returned.reshape(tok_rows, returned.shape[2] * returned.shape[3])
    mixed = jnp.dot(
        flat_rows,
        lax.all_gather(out_weight, "dp", axis=1, tiled=True),
        preferred_element_type=jnp.float32,
    ).astype(jnp.bfloat16)
    return mixed[None]


def solution(mesh):
    return jax.shard_map(
        body,
        mesh=mesh,
        in_specs=(
            P(("grp", "dp"), "sp", None, None),
            P(("grp", "dp"), "sp", None),
            P(("grp", "dp"), "sp", None),
            P(),
            P("dp", "sp"),
            P(None, "dp"),
        ),
        out_specs=P(("grp", "dp"), "sp", None),
        check_vma=False,
    )
```

profile of v0, /device:TPU:0, one launch (start us, length us, event | category | flops | bytes accessed | tf_op | source)
XLA Modules:
  0.0 100.5 jit_solution(13270757476425511561)
XLA Ops:
  6.5 0.0 copy-start
  6.5 0.0 copy-start.2
  6.5 0.0 all-gather.3.cloned.1.call-start
  6.5 0.7 all-gather.3.cloned.1.call-update
  7.3 0.0 all-gather.5.cloned.1.call-start
  7.3 0.7 all-gather.5.cloned.1.call-update
  8.0 1.1 %slice.33 = bf16[1,128,16,128]{1,3,0,2:T(8,128)(2,1)S(1)} slice(bf16[1,128,16,192]{1,3,0,2:T(8,128)(2,1)} %bitcast.45), slice={[0:1], [0:128], [0:16], [0:128]} | slice | bytes 1048576 | tf_op jit(solution)/shard_map/slice | solution.py:67
  9.1 0.9 fusion.29
  10.0 1.0 slice_bitcast_fusion
  11.0 0.1 fusion.23
  11.1 0.9 pad_maximum_fusion
  12.0 6.3 %all-to-all-start = ((bf16[1,128,16,192]{1,3,0,2:T(8,128)(2,1)}), bf16[1,128,16,192]{1,3,0,2:T(8,128)(2,1)S(1)}, u32[]{:S(2)}, u32[]{:S(2)}) async-start(bf16[1,128,16,192]{1,3,0,2:T(8,128)(2,1)} %pad_maximum_fusion), calls=%async_computation | async-start | bytes 1572864 | tf_op jit(solution)/shard_map/all_to_all | solution.py:69
  18.4 25.7 %all_gather.14 = bf16[1,512,64]{1,2,0:T(8,128)(2,1)S(1)} all-gather(bf16[1,128,64]{1,2,0:T(8,128)(2,1)S(1)} %pad_maximum_fusion.1), channel_id=1, replica_groups=mesh['grp'=2,'sp'=4,'dp'=4] {'sp'}, dimensions={1}, use_global_device_ids=true | all-gather | bytes 81920 | tf_op jit(solution)/shard_map/all_gather | solution.py:72
  44.1 0.8 iota_compare_fusion
  44.9 0.0 copy-done
  44.9 0.1 fusion.15
  45.0 0.0 copy-done.2
  45.0 0.1 fusion.17
  45.1 14.7 %all_gather.12 = bf16[1,512,512]{2,1,0:T(8,128)(2,1)S(1)} all-gather(bf16[1,128,512]{2,1,0:T(8,128)(2,1)S(1)} %fusion.17), channel_id=1, replica_groups=mesh['grp'=2,'sp'=4,'dp'=4] {'sp'}, dimensions={1}, use_global_device_ids=true | all-gather | bytes 655360 | tf_op jit(solution)/shard_map/all_gather | solution.py:71
  59.8 0.0 all-to-all-done
  59.8 0.6 copy.35
  60.4 0.3 squeeze.21
  60.7 0.0 all-gather.3.cloned.1.call-done
  60.7 1.9 %convolution_convert_fusion.1 = bf16[512,1024]{1,0:T(8,128)(2,1)S(1)} fusion(bf16[512,1024]{1,0:T(8,128)(2,1)} %all-gather.3.cloned.1.call-done, bf16[1,512,512]{2,1,0:T(8,128)(2,1)S(1)} %all_gather.12), kind=kOutput, calls=%fused_computation.11 | convolution fusion | flops 537395200 | bytes 2621440 | tf_op jit(solution)/shard_map/dot_general | solution.py:75
  62.7 0.0 copy-start.1
  62.7 0.5 copy.33
  63.3 0.8 fusion.9
  64.1 0.0 copy-done.1
  64.2 2.1 %fusion.33 = (f32[4,512]{1,0:T(4,128)S(1)}, f32[4,512,512]{1,2,0:T(8,128)S(1)}) fusion(f32[4,512,512]{1,2,0:T(8,128)S(1)} %fusion.9, pred[512,512]{0,1:T(8,128)(4,1)S(1)} %copy-done.1), kind=kOutput, calls=%fused_computation.58 | output fusion | flops 6291967 | bytes 8658944 | tf_op jit(solution)/shard_map/while/body/eval_jaxpr/sub | solution.py:45
  66.3 0.5 fusion.8
  66.8 0.3 copy.29
  67.1 13.6 %all_to_all.30 = bf16[1,512,4,128]{3,2,0,1:T(4,128)(2,1)S(1)} all-to-all(bf16[1,512,4,128]{3,2,0,1:T(4,128)(2,1)S(1)} %copy.29), channel_id=1, replica_groups=mesh['grp'=2,'sp'=4,'dp'=4] {'sp'}, dimensions={1} | all-to-all | bytes 1048576 | tf_op jit(solution)/shard_map/all_to_all | solution.py:82
  80.8 0.1 copy.30
  80.8 0.3 copy.31
  81.1 7.1 %all-gather.5.cloned.1.call-done = bf16[2048,2048]{1,0:T(8,128)(2,1)} async-done(((bf16[2048,512]{1,0:T(8,128)(2,1)}), bf16[2048,2048]{1,0:T(8,128)(2,1)}) %all-gather.5.cloned.1.call-update) | async-done | bytes 8388624 | tf_op jit(solution)/shard_map/all_gather | solution.py:86
  88.2 5.5 %fusion.2 = bf16[1,128,2048]{2,1,0:T(8,128)(2,1)} fusion(bf16[128,2048]{0,1:T(8,128)(2,1)S(1)} %bitcast.39, bf16[2048,2048]{1,0:T(8,128)(2,1)} %all-gather.5.cloned.1.call-done), kind=kOutput, calls=%fused_computation.6 | convolution fusion | flops 1074003968 | bytes 9437184 | tf_op jit(solution)/shard_map/dot_general | solution.py:84
  (6 shorter events, 0.1 us)
Async XLA Ops:
  6.5 38.3 %copy-start = (bf16[1,128,512]{2,1,0:T(8,128)(2,1)S(1)}, bf16[1,128,512]{2,1,0:T(8,128)(2,1)}, u32[]{:S(2)}) copy-start(bf16[1,128,512]{2,1,0:T(8,128)(2,1)} %param.7) | copy-start | bytes 393220
  6.5 38.5 %copy-start.2 = (f32[512]{0:T(512)S(1)}, f32[512]{0:T(512)}, u32[]{:S(2)}) copy-start(f32[512]{0:T(512)} %param.9) | copy-start | bytes 6148
  6.5 54.2 %all-gather.3.cloned.1.call-start = ((), (), s32[]{:S(2)}) async-start(), calls=%async_computation.2 | async-start | bytes 1310720 | tf_op jit(solution)/shard_map/all_gather | solution.py:77
  7.3 80.9 %all-gather.5.cloned.1.call-start = ((), (), s32[]{:S(2)}) async-start(), calls=%async_computation.3 | async-start | bytes 10485760 | tf_op jit(solution)/shard_map/all_gather | solution.py:86
  12.0 47.8 %all-to-all-start = ((bf16[1,128,16,192]{1,3,0,2:T(8,128)(2,1)}), bf16[1,128,16,192]{1,3,0,2:T(8,128)(2,1)S(1)}, u32[]{:S(2)}, u32[]{:S(2)}) async-start(bf16[1,128,16,192]{1,3,0,2:T(8,128)(2,1)} %pad_maximum_fusion), calls=%async_computation | async-start | bytes 1572864 | tf_op jit(solution)/shard_map/all_to_all | solution.py:69
  62.7 1.5 %copy-start.1 = (pred[512,512]{0,1:T(8,128)(4,1)S(1)}, pred[512,512]{0,1:T(8,128)(4,1)}, u32[]{:S(2)}) copy-start(pred[512,512]{0,1:T(8,128)(4,1)} %iota_compare_fusion) | copy-start | bytes 786436
Sparse Core Ops, SparseCore 0:
  8.9 19.4 all-gather.2
  29.9 58.2 all-gather.4
where the time goes:
time: 101 us; the launch traced here: 100 us
  blocking collectives  54 us (53%)
  between operations  13.6 us (13%)
  matrix products  8.7 us (9%)
  waiting for transfers between devices  8.51 us (8%)
  starting transfers between devices  6.39 us (6%)
  other arithmetic  5.05 us (5%)
  local copies, waits for them, and re-layouts  4.24 us (4%)
    all_gather x1, blocking collectives, body(): lax.all_gather(key_rot[None], 'sp', axis=1, tiled=True)  25.7 us
    all_gather x1, blocking collectives, body(): lax.all_gather(latent_n[None], 'sp', axis=1, tiled=True)  14.7 us
    all_to_all x1, blocking collectives, body(): lax.all_to_all(attended[None], 'sp', split_axis=1, concat_axis=2, tiled=T...  13.6 us
    all_gather x1, waiting for transfers between devices, body(): lax.all_gather(out_weight, 'dp', axis=1, tiled=True)  7.08 us
    all_to_all x1, starting transfers between devices, body(): lax.all_to_all(query_rot[None], 'sp', split_axis=2, concat_axis=1, tiled=...  6.35 us
    dot_general x1, matrix products, body(): jnp.dot(flat_rows, lax.all_gather(out_weight, 'dp', axis=1, tiled=True),...  5.45 us
    sub x1, other arithmetic, one_block(): expo = jnp.exp(scores - top)  2.15 us
  transfers between devices with their start and end apart: 3, of which 1 were waited for; matrix products, arithmetic and copies ran while one was open for 12% of the time, Pallas kernels for 0%

commit v1 on v0

--- a/solution.py
+++ b/solution.py
@@ -1,3 +1,4 @@
+import functools
 import jax
 import jax.numpy as jnp
 from jax import lax
@@ -5,6 +6,18 @@
 
 NOPE = 128
 VD = 128
+
+
+def _run_domain(block_in, group_axis):
+    return jnp.concatenate(
+        jax.lax.all_to_all(
+            jnp.stack(jnp.split(block_in, jax.lax.axis_size(group_axis), axis=1)), group_axis, 0, 0
+        ),
+        axis=2,
+    )
+
+
+expand_spot = functools.partial(_run_domain, group_axis="sp")
 
 
 def rotate(values, positions):
@@ -79,7 +92,7 @@
     ).astype(jnp.bfloat16)
     kv_heads = kv_heads.reshape(whole_latent.shape[0], kv_weight.shape[1] // (NOPE + VD), NOPE + VD)
     attended = attend(query_heads[0], kv_heads, every_key[0])
-    returned = lax.all_to_all(attended[None], "sp", split_axis=1, concat_axis=2, tiled=True)
+    returned = expand_spot(attended[None])
     flat_rows = returned.reshape(tok_rows, returned.shape[2] * returned.shape[3])
     mixed = jnp.dot(
         flat_rows,

time: 101 us -> 101 us (level)
  no operation moved by 1% of the time
where the time goes in v1:
time: 101 us; the launch traced here: 100 us
  blocking collectives  54 us (53%)
  between operations  13.6 us (13%)
  waiting for transfers between devices  8.96 us (9%)
  matrix products  8.7 us (9%)
  starting transfers between devices  6.39 us (6%)
  other arithmetic  5.14 us (5%)
  local copies, waits for them, and re-layouts  3.7 us (4%)
    all_gather x1, blocking collectives, body(): lax.all_gather(key_rot[None], 'sp', axis=1, tiled=True)  25.7 us
    all_gather x1, blocking collectives, body(): lax.all_gather(latent_n[None], 'sp', axis=1, tiled=True)  14.7 us
    all_to_all x1, blocking collectives, _run_domain(): jax.lax.all_to_all(jnp.stack(jnp.split(block_in, jax.lax.axis_size(group_...  13.6 us
    all_gather x1, waiting for transfers between devices, body(): lax.all_gather(out_weight, 'dp', axis=1, tiled=True)  7.53 us
    all_to_all x1, starting transfers between devices, body(): lax.all_to_all(query_rot[None], 'sp', split_axis=2, concat_axis=1, tiled=...  6.35 us
    dot_general x1, matrix products, body(): jnp.dot(flat_rows, lax.all_gather(out_weight, 'dp', axis=1, tiled=True),...  5.45 us
    sub x1, other arithmetic, one_block(): expo = jnp.exp(scores - top)  2.15 us
  transfers between devices with their start and end apart: 3, of which 1 were waited for; matrix products, arithmetic and copies ran while one was open for 12% of the time, Pallas kernels for 0%

profile of v1, /device:TPU:0, one launch (start us, length us, event | category | flops | bytes accessed | tf_op | source)
XLA Modules:
  0.0 100.5 jit_solution(15954829376941877631)
XLA Ops:
  6.5 0.0 copy-start
  6.5 0.0 copy-start.2
  6.5 0.0 all-gather.3.cloned.1.call-start
  6.5 0.7 all-gather.3.cloned.1.call-update
  7.3 0.0 all-gather.5.cloned.1.call-start
  7.3 0.7 all-gather.5.cloned.1.call-update
  8.0 1.1 %slice.33 = bf16[1,128,16,128]{1,3,0,2:T(8,128)(2,1)S(1)} slice(bf16[1,128,16,192]{1,3,0,2:T(8,128)(2,1)} %bitcast.51), slice={[0:1], [0:128], [0:16], [0:128]} | slice | bytes 1048576 | tf_op jit(solution)/shard_map/slice | solution.py:80
  9.1 0.9 fusion.29
  10.0 1.0 slice_bitcast_fusion
  11.0 0.1 fusion.23
  11.1 1.0 pad_maximum_fusion
  12.0 6.3 %all-to-all-start = ((bf16[1,128,16,192]{1,3,0,2:T(8,128)(2,1)}), bf16[1,128,16,192]{1,3,0,2:T(8,128)(2,1)S(1)}, u32[]{:S(2)}, u32[]{:S(2)}) async-start(bf16[1,128,16,192]{1,3,0,2:T(8,128)(2,1)} %pad_maximum_fusion), calls=%async_computation | async-start | bytes 1572864 | tf_op jit(solution)/shard_map/all_to_all | solution.py:82
  18.4 25.7 %all_gather.14 = bf16[1,512,64]{1,2,0:T(8,128)(2,1)S(1)} all-gather(bf16[1,128,64]{1,2,0:T(8,128)(2,1)S(1)} %pad_maximum_fusion.2), channel_id=1, replica_groups=mesh['grp'=2,'sp'=4,'dp'=4] {'sp'}, dimensions={1}, use_global_device_ids=true | all-gather | bytes 81920 | tf_op jit(solution)/shard_map/all_gather | solution.py:85
  44.1 0.8 iota_compare_fusion
  44.9 0.0 copy-done
  44.9 0.1 fusion.15
  45.0 0.0 copy-done.2
  45.0 0.1 fusion.17
  45.1 14.7 %all_gather.12 = bf16[1,512,512]{2,1,0:T(8,128)(2,1)S(1)} all-gather(bf16[1,128,512]{2,1,0:T(8,128)(2,1)S(1)} %fusion.17), channel_id=1, replica_groups=mesh['grp'=2,'sp'=4,'dp'=4] {'sp'}, dimensions={1}, use_global_device_ids=true | all-gather | bytes 655360 | tf_op jit(solution)/shard_map/all_gather | solution.py:84
  59.8 0.0 all-to-all-done
  59.8 0.6 copy.20
  60.4 0.3 squeeze.21
  60.7 0.0 all-gather.3.cloned.1.call-done
  60.8 1.9 %convolution_convert_fusion.1 = bf16[512,1024]{1,0:T(8,128)(2,1)S(1)} fusion(bf16[512,1024]{1,0:T(8,128)(2,1)} %all-gather.3.cloned.1.call-done, bf16[1,512,512]{2,1,0:T(8,128)(2,1)S(1)} %all_gather.12), kind=kOutput, calls=%fused_computation.11 | convolution fusion | flops 537395200 | bytes 2621440 | tf_op jit(solution)/shard_map/dot_general | solution.py:88
  62.7 0.0 copy-start.1
  62.7 0.5 copy.18
  63.3 0.8 fusion.9
  64.2 0.0 copy-done.1
  64.2 2.1 %fusion.33 = (f32[4,512]{1,0:T(4,128)S(1)}, f32[4,512,512]{1,2,0:T(8,128)S(1)}) fusion(f32[4,512,512]{1,2,0:T(8,128)S(1)} %fusion.9, pred[512,512]{0,1:T(8,128)(4,1)S(1)} %copy-done.1), kind=kOutput, calls=%fused_computation.63 | output fusion | flops 6291967 | bytes 8658944 | tf_op jit(solution)/shard_map/while/body/eval_jaxpr/sub | solution.py:58
  66.3 0.5 fusion.8
  66.8 0.1 slice_bitcast_fusion.4
  66.9 0.1 pad_maximum_fusion.1
  67.0 13.6 %all_to_all.20 = bf16[4,1,128,4,128]{2,4,3,1,0:T(8,128)(2,1)S(1)} all-to-all(bf16[4,1,128,4,128]{2,4,3,1,0:T(8,128)(2,1)S(1)} %pad_maximum_fusion.1), channel_id=1, replica_groups=mesh['grp'=2,'sp'=4,'dp'=4] {'sp'}, dimensions={0} | all-to-all | bytes 1048576 | tf_op jit(solution)/shard_map/all_to_all | solution.py:13
  80.7 7.5 %all-gather.5.cloned.1.call-done = bf16[2048,2048]{1,0:T(8,128)(2,1)} async-done(((bf16[2048,512]{1,0:T(8,128)(2,1)}), bf16[2048,2048]{1,0:T(8,128)(2,1)}) %all-gather.5.cloned.1.call-update) | async-done | bytes 8388624 | tf_op jit(solution)/shard_map/all_gather | solution.py:99
  88.2 5.5 %fusion.2 = bf16[1,128,2048]{2,1,0:T(8,128)(2,1)} fusion(bf16[128,2048]{0,1:T(8,128)(2,1)S(1)} %bitcast.46, bf16[2048,2048]{1,0:T(8,128)(2,1)} %all-gather.5.cloned.1.call-done), kind=kOutput, calls=%fused_computation.6 | convolution fusion | flops 1074003968 | bytes 9437184 | tf_op jit(solution)/shard_map/dot_general | solution.py:97
  (6 shorter events, 0.1 us)
Async XLA Ops:
  6.5 38.4 %copy-start = (bf16[1,128,512]{2,1,0:T(8,128)(2,1)S(1)}, bf16[1,128,512]{2,1,0:T(8,128)(2,1)}, u32[]{:S(2)}) copy-start(bf16[1,128,512]{2,1,0:T(8,128)(2,1)} %param.7) | copy-start | bytes 393220
  6.5 38.5 %copy-start.2 = (f32[512]{0:T(512)S(1)}, f32[512]{0:T(512)}, u32[]{:S(2)}) copy-start(f32[512]{0:T(512)} %param.9) | copy-start | bytes 6148
  6.5 54.2 %all-gather.3.cloned.1.call-start = ((), (), s32[]{:S(2)}) async-start(), calls=%async_computation.2 | async-start | bytes 1310720 | tf_op jit(solution)/shard_map/all_gather | solution.py:90
  7.3 80.9 %all-gather.5.cloned.1.call-start = ((), (), s32[]{:S(2)}) async-start(), calls=%async_computation.3 | async-start | bytes 10485760 | tf_op jit(solution)/shard_map/all_gather | solution.py:99
  12.0 47.8 %all-to-all-start = ((bf16[1,128,16,192]{1,3,0,2:T(8,128)(2,1)}), bf16[1,128,16,192]{1,3,0,2:T(8,128)(2,1)S(1)}, u32[]{:S(2)}, u32[]{:S(2)}) async-start(bf16[1,128,16,192]{1,3,0,2:T(8,128)(2,1)} %pad_maximum_fusion), calls=%async_computation | async-start | bytes 1572864 | tf_op jit(solution)/shard_map/all_to_all | solution.py:82
  62.7 1.5 %copy-start.1 = (pred[512,512]{0,1:T(8,128)(4,1)S(1)}, pred[512,512]{0,1:T(8,128)(4,1)}, u32[]{:S(2)}) copy-start(pred[512,512]{0,1:T(8,128)(4,1)} %iota_compare_fusion) | copy-start | bytes 786436
Sparse Core Ops, SparseCore 0:
  8.9 19.4 all-gather.2
  29.9 58.2 all-gather.4
